TPU v7x, 32 devices: a whole 2x2x4 slice. The times are simulated.
32 devices in a mesh: sp: 8 (over z, y), fs: 2 (over x), tp: 2 (over core).
Axes of the slice: x: 2, y: 2, z: 4, core: 2. Of those that a mesh axis runs over, the one named last changes fastest.
Arguments:
- tokens: bfloat16 [8192, 2048], P(('fs', 'sp', 'tp')), parts along dimension 0, may hold values from -60 to 60
- norm_gain: float32 [2048], replicated, may hold values from 0.1 to 1.9
- pool_in: bfloat16 [2048, 512], P('sp', 'tp'), may hold values from -0.125 to 0.125
- gate_in: bfloat16 [2048, 1024], P('sp', 'tp'), may hold values from -0.125 to 0.125
- value_in: bfloat16 [2048, 1024], P('sp', 'tp'), may hold values from -0.125 to 0.125
- pool_mix: bfloat16 [4, 128, 128], P('tp'), may hold values from -0.5 to 0.5
- averaging_factor: float32 [512], P('tp'), may hold values from 0.25 to 0.75
- conv_taps: float32 [4, 1024], P(None, 'tp'), may hold values from -3 to 3
- rate_mix: bfloat16 [16, 64, 64], P('tp'), may hold values from -0.75 to 0.75
- input_mix: bfloat16 [16, 64, 64], P('tp'), may hold values from -0.75 to 0.75
- log_rate: float32 [1024], P('tp'), may hold values from 1.5 to 16
- decay_shift: float32 [32, 4096], P(('fs', 'tp'), 'sp'), parts along dimension 0, may hold values from -1.1 to 0
- initial_state: float32 [2048], P(('fs', 'tp')), parts along dimension 0, may hold values from -6 to 6
- out_pool: bfloat16 [2048, 512], P('sp', 'tp'), may hold values from -0.15625 to 0.15625
- out_rnn: bfloat16 [2048, 1024], P('sp', 'tp'), may hold values from -0.15625 to 0.15625
Outputs:
- mixed: bfloat16 [8192, 2048], P(('fs', 'sp', 'tp')), parts along dimension 0
There are 2 independent parts, one for each index of `fs`. A program takes and returns all parts, laid end to end along the dimension named above; an argument that names none is the same for every part. Nothing has to cross between parts.
All inputs are finite; a program needn't handle non-finite values.
Results may differ from a plain program's by a relative error of at most 0.012.
Values may be sent and summed in bfloat16 or wider, within the bound.
A program may use at most 64 MiB of HBM per device.

v0:
```python
import jax
import jax.numpy as jnp
from jax import lax
from jax.sharding import PartitionSpec as P

GROUP_WIDTH = 128
HEAD_DIM = 64
TAPS = 4
REACH = 16


epsilon = 1e-06
sharpness = 8.0


def from_behind(value, axis, steps):
    count = lax.axis_size(axis)
    first, last = (max(0, -steps), min(count, count - steps))
    return lax.ppermute(value, axis, [(source, source + steps) for source in range(first, last)])


def carried_in(array, axis, combine, identity):
    count, index = (lax.axis_size(axis), lax.axis_index(axis))
    everything = jax.tree.map(lambda part: lax.all_gather(part, axis), array)
    start = jax.tree.map(
        lambda part, zero: jnp.broadcast_to(jnp.asarray(zero, part.dtype), part.shape),
        array,
        identity,
    )

    def hop(k, before):
        reached = k < index
        new = combine(before, jax.tree.map(lambda part: part[k], everything))
        return jax.tree.map(lambda a, b: jnp.where(reached, a, b), new, before)

    return lax.fori_loop(0, count, hop, start)


def chain_pairs(first_pair, second_pair):
    return (first_pair[0] * second_pair[0], second_pair[0] * first_pair[1] + second_pair[1])


def right_product(left_rows, weight_rows):
    return lax.dot_general(
        left_rows, weight_rows, (((1,), (1,)), ((), ())), preferred_element_type=jnp.float32
    )


def shards(
    tokens,
    norm_gain,
    pool_in,
    gate_in,
    value_in,
    pool_mix,
    averaging_factor,
    conv_taps,
    rate_mix,
    input_mix,
    log_rate,
    decay_shift,
    initial_state,
    out_pool,
    out_rnn,
):
    tp_index = lax.axis_index("tp")
    sp_index = lax.axis_index("sp")
    gathered = (
        lax.all_gather(pool_in, "sp", axis=0, tiled=True),
        lax.all_gather(gate_in, "sp", axis=0, tiled=True),
        lax.all_gather(value_in, "sp", axis=0, tiled=True),
        lax.all_gather(out_pool, "sp", axis=0, tiled=True),
        lax.all_gather(out_rnn, "sp", axis=0, tiled=True),
    )
    pool_weight, gate_weight, value_weight, averaging_exit_matrix, out_rnn_weight = gathered
    pool_width = pool_weight.shape[1]
    rnn_width = gate_weight.shape[1]
    widened = lax.all_gather(tokens, "tp", axis=0, tiled=True).astype(jnp.float32)
    scaling = lax.rsqrt(jnp.mean(widened * widened, axis=1, keepdims=True) + epsilon)
    normed = (widened * scaling * norm_gain[None, :]).astype(jnp.bfloat16)
    outputs = [
        jnp.dot(normed, matrix, preferred_element_type=jnp.float32).astype(jnp.bfloat16)
        for matrix in (pool_weight, gate_weight, value_weight)
    ]
    projected = jnp.concatenate(outputs, axis=1)
    block_rows = projected.shape[0]
    pool_pre = projected[:, :pool_width]
    gate_pre = projected[:, pool_width : pool_width + rnn_width]
    value_pre = projected[:, pool_width + rnn_width :]
    edge_rows = jnp.concatenate(
        [pool_pre[block_rows - REACH :], value_pre[block_rows - REACH :]], axis=1
    )
    earlier_rows = from_behind(edge_rows, "sp", 1)
    pool_values = pool_pre.astype(jnp.float32)
    pool_padded = jnp.concatenate([earlier_rows[:, :pool_width], pool_pre], axis=0).astype(
        jnp.float32
    )
    value_padded = jnp.concatenate([earlier_rows[:, pool_width:], value_pre], axis=0).astype(
        jnp.float32
    )
    groups_here = pool_width // GROUP_WIDTH
    group_index = tp_index * groups_here + jnp.arange(pool_width, dtype=jnp.int32) // GROUP_WIDTH
    window = jnp.left_shift(jnp.int32(2), group_index)
    positions = sp_index * block_rows + jnp.arange(block_rows, dtype=jnp.int32)
    window_sum = jnp.zeros((block_rows, pool_width), jnp.float32)
    for steps_back in range(REACH):
        lagged = pool_padded[REACH - steps_back : REACH - steps_back + block_rows]
        window_sum = window_sum + jnp.where(steps_back < window[None, :], lagged, 0.0)
    counts = jnp.minimum(positions[:, None] + 1, window[None, :]).astype(jnp.float32)
    pooled = (window_sum / counts - pool_values).astype(jnp.bfloat16)
    grouped = pooled.reshape(block_rows, groups_here, GROUP_WIDTH)
    mixed_groups = jnp.einsum("tgc,gcd->tgd", grouped, pool_mix, preferred_element_type=jnp.float32)
    pool_out = (mixed_groups.reshape(block_rows, pool_width) * averaging_factor[None, :]).astype(
        jnp.bfloat16
    )
    start_row = REACH - TAPS + 1
    convolved = conv_taps[0][None, :] * value_padded[start_row : start_row + block_rows]
    for tap_index in range(1, TAPS):
        convolved = (
            convolved
            + conv_taps[tap_index][None, :]
            * value_padded[start_row + tap_index : start_row + tap_index + block_rows]
        )
    conv_out = convolved.astype(jnp.bfloat16)
    heads_here = rnn_width // HEAD_DIM
    both_mixes = jnp.concatenate([rate_mix, input_mix], axis=2)
    gate_terms = jnp.einsum(
        "thc,hcd->thd",
        conv_out.reshape(block_rows, heads_here, HEAD_DIM),
        both_mixes,
        preferred_element_type=jnp.float32,
    )
    rate_gate = jax.nn.sigmoid(gate_terms[:, :, :HEAD_DIM]).reshape(block_rows, rnn_width)
    input_gate = jax.nn.sigmoid(gate_terms[:, :, HEAD_DIM:]).reshape(block_rows, rnn_width)
    shifts = jnp.broadcast_to(
        jnp.transpose(decay_shift)[:, :, None], (block_rows, heads_here, HEAD_DIM)
    ).reshape(block_rows, rnn_width)
    log_decay = -sharpness * rate_gate * jax.nn.softplus(-log_rate)[None, :] + shifts
    decays = jnp.exp(log_decay)
    drives = jnp.sqrt(-jnp.expm1(2.0 * log_decay)) * input_gate * conv_out.astype(jnp.float32)
    cumulative, local_state = lax.associative_scan(chain_pairs, (decays, drives), axis=0)
    identity = (jnp.ones((rnn_width,), jnp.float32), jnp.zeros((rnn_width,), jnp.float32))
    prior_decay, prior_state = carried_in(
        (cumulative[block_rows - 1], local_state[block_rows - 1]), "sp", chain_pairs, identity
    )
    carried = prior_decay * initial_state + prior_state
    hidden_state = local_state + cumulative * carried[None, :]
    rnn_out = (jax.nn.gelu(gate_pre.astype(jnp.float32), approximate=True) * hidden_state).astype(
        jnp.bfloat16
    )
    return lax.psum_scatter(
        right_product(pool_out, averaging_exit_matrix) + right_product(rnn_out, out_rnn_weight),
        "tp",
        scatter_dimension=0,
        tiled=True,
    ).astype(jnp.bfloat16)


def solution(mesh):
    placed = (
        P(("fs", "sp", "tp"), None),
        P(),
        P("sp", "tp"),
        P("sp", "tp"),
        P("sp", "tp"),
        P("tp", None, None),
        P("tp"),
        P(None, "tp"),
        P("tp", None, None),
        P("tp", None, None),
        P("tp"),
        P(("fs", "tp"), "sp"),
        P(("fs", "tp")),
        P("sp", "tp"),
        P("sp", "tp"),
    )
    return jax.shard_map(
        shards, mesh=mesh, in_specs=placed, out_specs=P(("fs", "sp", "tp"), None), check_vma=False
    )
```

profile of v0, /device:TPU:0, one launch (start us, length us, event | category | flops | bytes accessed | tf_op | source)
XLA Modules:
  0.0 381.2 jit_solution(15395088567445469416)
XLA Ops:
  15.7 6.6 %all-gather.9.cloned.1.call-done = bf16[512,2048]{1,0:T(8,128)(2,1)} async-done(((bf16[256,2048]{1,0:T(8,128)(2,1)}), bf16[512,2048]{1,0:T(8,128)(2,1)}) %all-gather.9.cloned.1.call-update) | async-done | bytes 2097168 | tf_op jit(solution)/shard_map/all_gather | solution.py:78
  22.2 2.2 fusion
  24.5 41.4 %all-gather.11.cloned.1.call-done = bf16[2048,256]{1,0:T(8,128)(2,1)} async-done(((bf16[256,256]{1,0:T(8,128)(2,1)}), bf16[2048,256]{1,0:T(8,128)(2,1)}) %all-gather.11.cloned.1.call-update) | async-done | bytes 1048592 | tf_op jit(solution)/shard_map/all_gather | solution.py:69
  65.8 2.0 convolution_convert_fusion.2
  68.6 47.2 %all-gather.13.cloned.1.call-done = bf16[2048,512]{1,0:T(8,128)(2,1)} async-done(((bf16[256,512]{1,0:T(8,128)(2,1)}), bf16[2048,512]{1,0:T(8,128)(2,1)}) %all-gather.13.cloned.1.call-update) | async-done | bytes 2097168 | tf_op jit(solution)/shard_map/all_gather | solution.py:71
  115.8 2.9 convolution_convert_fusion.1
  119.5 2.6 collective-permute-start
  127.2 2.1 copy.30
  129.2 1.6 convolution_bitcast_fusion
  130.9 1.9 fusion.12
  132.8 2.5 copy.31
  135.3 2.6 copy.33
  137.9 4.4 %convert_multiply_fusion.5 = (f32[512,512]{1,0:T(8,128)}, f32[512,512]{1,0:T(8,128)}) fusion(f32[512,512]{1,0:T(8,128)} %copy.33, f32[512,512]{1,0:T(8,128)} %copy.32, f32[512,512]{1,0:T(8,128)} %copy.31, f32[512]{0:T(512)S(1)} %fusion.63, f32[528,512]{1,0:T(8,128)S(1)} %maximum_convert_fusion, f32[512]{0:T(512)S(1)} %bitcast.61, f32[512]{0:T(512)S(1)} %bitcast.63, ...), kind=kLoop, calls=%fused_computation.41 | loop fusion | flops 3932160 | bytes 9447424 | tf_op jit(solution)/shard_map/mul | solution.py:140
  142.2 3.7 slice.389
  146.0 3.6 slice.390
  149.6 2.1 slice.388
  151.7 2.1 slice.392
  153.7 2.7 multiply_add_fusion.1
  156.5 2.5 slice.395
  158.9 2.5 slice.396
  161.4 2.5 slice.394
  163.9 2.5 slice.398
  166.4 2.0 multiply_add_fusion.2
  171.4 1.6 slice.404
  173.0 1.9 multiply_add_fusion.3
  225.3 1.6 slice.399
  229.7 2.5 slice.393
  232.3 2.5 slice.450
  237.4 2.1 slice.387
  239.5 3.7 slice.452
  249.8 1.9 fusion.49
  253.7 4.6 %pad.127 = f32[512,512]{1,0:T(8,128)} pad(f32[256,512]{1,0:T(8,128)} %add.492, f32[]{:T(128)} %constant.117.clone.1), padding=1_0_1x0_0_0 | pad | bytes 1572868 | tf_op jit(solution)/shard_map/pad | solution.py:141
  258.3 1.7 pad_maximum_fusion.3
  260.0 2.6 pad.142
  262.6 1.6 pad.143
  264.3 2.1 add.502
  266.3 2.7 fusion.20
  269.9 4.6 %pad.126 = f32[512,512]{1,0:T(8,128)} pad(f32[256,512]{1,0:T(8,128)} %pad_maximum_fusion, f32[]{:T(128)} %constant.117.clone.1), padding=0_1_1x0_0_0 | pad | bytes 1572868 | tf_op jit(solution)/shard_map/pad | solution.py:141
  275.2 26.7 %all-gather.1 = f32[8,1,512]{2,1,0:T(1,128)S(1)} all-gather(f32[1,1,512]{2,1,0:T(1,128)S(1)} %add_bitcast_fusion), channel_id=1, replica_groups=mesh['sp'=8,'fs'=2,'tp'=2] {'sp'}, dimensions={0}, use_global_device_ids=true | all-gather | bytes 18432 | tf_op jit(solution)/shard_map/all_gather | solution.py:24
  301.9 4.7 %pad.145 = f32[512,512]{1,0:T(8,128)} pad(f32[256,512]{1,0:T(8,128)} %add.502, f32[]{:T(128)} %constant.117.clone.1), padding=1_0_1x0_0_0 | pad | bytes 1572868 | tf_op jit(solution)/shard_map/pad | solution.py:141
  306.6 1.9 pad_maximum_fusion.1
  308.6 4.6 %pad.144 = f32[512,512]{1,0:T(8,128)} pad(f32[256,512]{1,0:T(8,128)} %pad_maximum_fusion.1, f32[]{:T(128)} %constant.117.clone.1), padding=0_1_1x0_0_0 | pad | bytes 1572868 | tf_op jit(solution)/shard_map/pad | solution.py:141
  313.9 26.3 %all-gather = f32[8,1,512]{2,1,0:T(1,128)S(1)} all-gather(f32[1,1,512]{2,1,0:T(1,128)S(1)} %add_bitcast_fusion.1), channel_id=1, replica_groups=mesh['sp'=8,'fs'=2,'tp'=2] {'sp'}, dimensions={0}, use_global_device_ids=true | all-gather | bytes 18432 | tf_op jit(solution)/shard_map/all_gather | solution.py:24
  341.6 7.2 %fusion.46 = f32[2,512,128]{1,2,0:T(8,128)S(1)} fusion(bf16[2,128,128]{2,1,0:T(8,128)(2,1)S(1)} %copy-done, bf16[512,256]{1,0:T(8,128)(2,1)S(1)} %copy-done.8, s32[256]{0:T(256)S(1)} %copy-done.46, s32[512]{0:T(512)S(1)} %copy-done.42, f32[528,256]{1,0:T(8,128)} %maximum_convert_fusion.1, pred[256]{0:T(512)(128)(4,1)S(1)} %copy-done.47, ...), kind=kOutput, calls=%fused_computation.93 | convolution fusion | flops 38404096 | bytes 9250560 | tf_op jit(solution)/shard_map/tgc,gcd->tgd/dot_general | solution.py:112
  349.0 4.0 %fusion.77 = f32[512,2048]{1,0:T(8,128)} fusion(bf16[512,256]{0,1:T(8,128)(2,1)S(1)} %fusion.38, bf16[2048,256]{1,0:T(8,128)(2,1)} %all-gather.15.cloned.1.call-done), kind=kOutput, calls=%fused_computation.191 | convolution fusion | flops 536870912 | bytes 5505024 | tf_op jit(solution)/shard_map/dot_general | solution.py:44
  353.0 9.1 %convolution_add_fusion = f32[512,2048]{1,0:T(8,128)} fusion(f32[512,2048]{1,0:T(8,128)} %fusion.77, bf16[2048,512]{1,0:T(8,128)(2,1)} %all-gather.19.cloned.1.call-done, bf16[2048,512]{1,0:T(8,128)(2,1)} %all-gather.17.cloned.1.call-done, f32[512,512]{1,0:T(8,128)} %pad.144, f32[512,512]{1,0:T(8,128)} %pad.145, f32[512,512]{1,0:T(8,128)} %pad.126, ...), kind=kOutput, calls=%fused_computation.9 | convolution fusion | flops 2156920832 | bytes 18886656 | tf_op jit(solution)/shard_map/dot_general | solution.py:44
  362.2 9.4 %reduce-scatter.2.cloned.1.call-done = f32[256,2048]{1,0:T(8,128)} async-done(((f32[512,2048]{1,0:T(8,128)}), f32[256,2048]{1,0:T(8,128)}) %reduce-scatter.2.cloned.1.call-update) | async-done | bytes 2097168 | tf_op jit(solution)/shard_map/reduce_scatter | solution.py:151
  371.6 2.7 convert_element_type.63
  (282 shorter events, 86.5 us)
Async XLA Ops:
  6.5 335.0 %copy-start = (bf16[2,128,128]{2,1,0:T(8,128)(2,1)S(1)}, bf16[2,128,128]{2,1,0:T(8,128)(2,1)}, u32[]{:S(2)}) copy-start(bf16[2,128,128]{2,1,0:T(8,128)(2,1)} %param.22) | copy-start | bytes 196612
  6.5 8.5 %copy-start.37 = (f32[4,512]{1,0:T(4,128)S(1)}, f32[4,512]{1,0:T(4,128)}, u32[]{:S(2)}) copy-start(f32[4,512]{1,0:T(4,128)} %param.24) | copy-start | bytes 24580
  6.5 8.5 %copy-start.43 = (f32[512]{0:T(512)S(1)}, f32[512]{0:T(512)}, u32[]{:S(2)}) copy-start(f32[512]{0:T(512)} %param.27) | copy-start | bytes 6148
  6.5 59.3 %copy-start.23 = (f32[2048]{0:T(1024)S(1)}, f32[2048]{0:T(1024)}, u32[]{:S(2)}) copy-start(f32[2048]{0:T(1024)} %param.18) | copy-start | bytes 24580
  6.5 15.7 %all-gather.9.cloned.1.call-start = ((), (), s32[]{:S(2)}) async-start(), calls=%async_computation.1 | async-start | bytes 3145728 | tf_op jit(solution)/shard_map/all_gather | solution.py:78
  7.3 58.6 %all-gather.11.cloned.1.call-start = ((), (), s32[]{:S(2)}) async-start(), calls=%async_computation.2 | async-start | bytes 1179648 | tf_op jit(solution)/shard_map/all_gather | solution.py:69
  8.0 107.8 %all-gather.13.cloned.1.call-start = ((), (), s32[]{:S(2)}) async-start(), calls=%async_computation.3 | async-start | bytes 2359296 | tf_op jit(solution)/shard_map/all_gather | solution.py:71
  8.8 340.3 %all-gather.15.cloned.1.call-start = ((), (), s32[]{:S(2)}) async-start(), calls=%async_computation.4 | async-start | bytes 1179648 | tf_op jit(solution)/shard_map/all_gather | solution.py:72
  9.3 343.7 %all-gather.17.cloned.1.call-start = ((), (), s32[]{:S(2)}) async-start(), calls=%async_computation.5 | async-start | bytes 2359296 | tf_op jit(solution)/shard_map/all_gather | solution.py:70
  9.9 343.1 %all-gather.19.cloned.1.call-start = ((), (), s32[]{:S(2)}) async-start(), calls=%async_computation.6 | async-start | bytes 2359296 | tf_op jit(solution)/shard_map/all_gather | solution.py:73
  10.5 361.1 %reduce-scatter.2.cloned.1.call-start = ((), (), s32[]{:S(2)}) async-start(), calls=%async_computation.7 | async-start | bytes 6291456 | tf_op jit(solution)/shard_map/reduce_scatter | solution.py:151
  22.2 43.6 %copy-start.1 = (bf16[512,2048]{1,0:T(8,128)(2,1)S(1)}, bf16[512,2048]{1,0:T(8,128)(2,1)}, u32[]{:S(2)}) copy-start(bf16[512,2048]{1,0:T(8,128)(2,1)} %all-gather.9.cloned.1.call-done) | copy-start | bytes 6291460
  24.5 91.3 %copy-start.25 = (f32[512]{0:T(512)}, f32[512]{0:T(512)S(1)}, u32[]{:S(2)}) copy-start(f32[512]{0:T(512)S(1)} %add_rsqrt_fusion) | copy-start | bytes 6148
  68.6 54.1 %copy-start.20 = (f32[8,512]{1,0:T(8,128)S(1)}, f32[8,512]{1,0:T(8,128)}, u32[]{:S(2)}) copy-start(f32[8,512]{1,0:T(8,128)} %param.28) | copy-start | bytes 49156
  119.5 4.6 %collective-permute-start = (bf16[16,768]{1,0:T(8,128)(2,1)S(1)}, bf16[16,768]{1,0:T(8,128)(2,1)S(1)}, u32[]{:S(2)}, u32[]{:S(2)}) collective-permute-start(bf16[16,768]{1,0:T(8,128)(2,1)S(1)} %pad_maximum_fusion.10), channel_id=1, source_target_pairs={{0,4},{4,8},{8,12},{12,16},{16,20},{20,24},{24,28},{1,5},{5,9},{9,... | collective-permute-start | bytes 73736 | tf_op jit(solution)/shard_map/ppermute | solution.py:19
  142.2 7.4 %copy-start.2 = (f32[512,512]{1,0:T(8,128)S(1)}, f32[512,512]{1,0:T(8,128)}, u32[]{:S(2)}) copy-start(f32[512,512]{1,0:T(8,128)} %get-tuple-element.155) | copy-start | bytes 3145732
  229.6 15.5 %copy-start.38 = (f32[1,512]{1,0:T(1,128)S(1)}, f32[1,512]{1,0:T(1,128)}, u32[]{:S(2)}) copy-start(f32[1,512]{1,0:T(1,128)} %get-tuple-element.184) | copy-start | bytes 6148
  229.6 15.5 %copy-start.39 = (f32[1,512]{1,0:T(1,128)S(1)}, f32[1,512]{1,0:T(1,128)}, u32[]{:S(2)}) copy-start(f32[1,512]{1,0:T(1,128)} %get-tuple-element.185) | copy-start | bytes 6148
  229.6 15.5 %copy-start.40 = (f32[1,512]{1,0:T(1,128)S(1)}, f32[1,512]{1,0:T(1,128)}, u32[]{:S(2)}) copy-start(f32[1,512]{1,0:T(1,128)} %get-tuple-element.186) | copy-start | bytes 6148
  229.6 15.5 %copy-start.41 = (f32[1,512]{1,0:T(1,128)S(1)}, f32[1,512]{1,0:T(1,128)}, u32[]{:S(2)}) copy-start(f32[1,512]{1,0:T(1,128)} %get-tuple-element.187) | copy-start | bytes 6148
  229.6 15.5 %copy-start.22 = (f32[2,512]{1,0:T(2,128)S(1)}, f32[2,512]{1,0:T(2,128)}, u32[]{:S(2)}) copy-start(f32[2,512]{1,0:T(2,128)} %get-tuple-element.217) | copy-start | bytes 12292
  229.6 15.5 %copy-start.21 = (f32[2,512]{1,0:T(2,128)S(1)}, f32[2,512]{1,0:T(2,128)}, u32[]{:S(2)}) copy-start(f32[2,512]{1,0:T(2,128)} %get-tuple-element.216) | copy-start | bytes 12292
  229.6 15.6 %copy-start.18 = (f32[3,512]{1,0:T(4,128)S(1)}, f32[3,512]{1,0:T(4,128)}, u32[]{:S(2)}) copy-start(f32[3,512]{1,0:T(4,128)} %slice.423) | copy-start | bytes 18436
  229.6 15.6 %copy-start.19 = (f32[3,512]{1,0:T(4,128)S(1)}, f32[3,512]{1,0:T(4,128)}, u32[]{:S(2)}) copy-start(f32[3,512]{1,0:T(4,128)} %slice.440) | copy-start | bytes 18436
  229.7 15.6 %copy-start.36 = (f32[1,512]{1,0:T(1,128)S(1)}, f32[1,512]{1,0:T(1,128)}, u32[]{:S(2)}) copy-start(f32[1,512]{1,0:T(1,128)} %slice.533) | copy-start | bytes 6148
  229.7 15.7 %copy-start.35 = (f32[1,512]{1,0:T(1,128)S(1)}, f32[1,512]{1,0:T(1,128)}, u32[]{:S(2)}) copy-start(f32[1,512]{1,0:T(1,128)} %slice.504) | copy-start | bytes 6148
  229.7 15.7 %copy-start.16 = (f32[7,512]{1,0:T(8,128)S(1)}, f32[7,512]{1,0:T(8,128)}, u32[]{:S(2)}) copy-start(f32[7,512]{1,0:T(8,128)} %slice.442) | copy-start | bytes 43012
  229.7 15.8 %copy-start.34 = (f32[1,512]{1,0:T(1,128)S(1)}, f32[1,512]{1,0:T(1,128)}, u32[]{:S(2)}) copy-start(f32[1,512]{1,0:T(1,128)} %slice.532) | copy-start | bytes 6148
  229.7 15.8 %copy-start.33 = (f32[1,512]{1,0:T(1,128)S(1)}, f32[1,512]{1,0:T(1,128)}, u32[]{:S(2)}) copy-start(f32[1,512]{1,0:T(1,128)} %slice.503) | copy-start | bytes 6148
  229.7 15.9 %copy-start.12 = (f32[15,512]{1,0:T(8,128)S(1)}, f32[15,512]{1,0:T(8,128)}, u32[]{:S(2)}) copy-start(f32[15,512]{1,0:T(8,128)} %slice.411) | copy-start | bytes 92164
  229.7 15.9 %copy-start.13 = (f32[15,512]{1,0:T(8,128)S(1)}, f32[15,512]{1,0:T(8,128)}, u32[]{:S(2)}) copy-start(f32[15,512]{1,0:T(8,128)} %slice.444) | copy-start | bytes 92164
  237.4 9.7 %copy-start.9 = (f32[31,512]{1,0:T(8,128)S(1)}, f32[31,512]{1,0:T(8,128)}, u32[]{:S(2)}) copy-start(f32[31,512]{1,0:T(8,128)} %slice.446) | copy-start | bytes 190468
  251.8 6.5 %copy-start.29 = (f32[1,512]{1,0:T(1,128)S(1)}, f32[1,512]{1,0:T(1,128)}, u32[]{:S(2)}) copy-start(f32[1,512]{1,0:T(1,128)} %slice.528) | copy-start | bytes 6148
  269.0 5.5 %copy-start.3 = (f32[512,512]{1,0:T(8,128)S(1)}, f32[512,512]{1,0:T(8,128)}, u32[]{:S(2)}) copy-start(f32[512,512]{1,0:T(8,128)} %pad.127) | copy-start | bytes 3145732
  269.0 37.6 %copy-start.27 = (f32[1,512]{1,0:T(1,128)S(1)}, f32[1,512]{1,0:T(1,128)}, u32[]{:S(2)}) copy-start(f32[1,512]{1,0:T(1,128)} %slice.527) | copy-start | bytes 6148
  301.9 38.4 %copy-start.8 = (bf16[512,256]{1,0:T(8,128)(2,1)S(1)}, bf16[512,256]{1,0:T(8,128)(2,1)}, u32[]{:S(2)}) copy-start(bf16[512,256]{1,0:T(8,128)(2,1)} %copy-done.7) | copy-start | bytes 786436
  301.9 38.4 %slice-start = ((bf16[16,768]{1,0:T(8,128)(2,1)}), bf16[16,256]{1,0:T(8,128)(2,1)S(1)}, s32[]{:S(2)}) async-start(bf16[16,768]{1,0:T(8,128)(2,1)} %copy-done.17), calls=%async_computation.8 | async-start | bytes 16384 | tf_op jit(solution)/shard_map/slice | solution.py:95
  306.6 34.5 %copy-start.14 = (f32[512]{0:T(512)S(1)}, f32[512]{0:T(512)}, u32[]{:S(2)}) copy-start(f32[512]{0:T(512)} %custom-call) | copy-start | bytes 6148
  306.6 34.5 %copy-start.15 = (f32[512]{0:T(512)S(1)}, f32[512]{0:T(512)}, u32[]{:S(2)}) copy-start(f32[512]{0:T(512)} %custom-call.1) | copy-start | bytes 6148
  306.6 34.9 %copy-start.44 = (f32[512]{0:T(512)S(1)}, f32[512]{0:T(512)}, u32[]{:S(2)}) copy-start(f32[512]{0:T(512)} %param.29) | copy-start | bytes 6148
  306.6 35.0 %copy-start.42 = (s32[512]{0:T(512)S(1)}, s32[512]{0:T(512)}, u32[]{:S(2)}) copy-start(s32[512]{0:T(512)} %add_add_fusion) | copy-start | bytes 6148
  306.6 35.0 %copy-start.46 = (s32[256]{0:T(256)S(1)}, s32[256]{0:T(256)}, u32[]{:S(2)}) copy-start(s32[256]{0:T(256)} %fusion.65) | copy-start | bytes 3076
  306.6 35.0 %copy-start.47 = (pred[256]{0:T(512)(128)(4,1)S(1)}, pred[256]{0:T(512)(128)(4,1)}, u32[]{:S(2)}) copy-start(pred[256]{0:T(512)(128)(4,1)} %get-tuple-element.200) | copy-start | bytes 772
  306.6 35.0 %copy-start.48 = (pred[256]{0:T(512)(128)(4,1)S(1)}, pred[256]{0:T(512)(128)(4,1)}, u32[]{:S(2)}) copy-start(pred[256]{0:T(512)(128)(4,1)} %get-tuple-element.201) | copy-start | bytes 772
  306.6 35.0 %copy-start.49 = (pred[256]{0:T(512)(128)(4,1)S(1)}, pred[256]{0:T(512)(128)(4,1)}, u32[]{:S(2)}) copy-start(pred[256]{0:T(512)(128)(4,1)} %get-tuple-element.202) | copy-start | bytes 772
  306.6 35.0 %copy-start.50 = (pred[256]{0:T(512)(128)(4,1)S(1)}, pred[256]{0:T(512)(128)(4,1)}, u32[]{:S(2)}) copy-start(pred[256]{0:T(512)(128)(4,1)} %get-tuple-element.203) | copy-start | bytes 772
  306.6 35.0 %copy-start.51 = (pred[256]{0:T(512)(128)(4,1)S(1)}, pred[256]{0:T(512)(128)(4,1)}, u32[]{:S(2)}) copy-start(pred[256]{0:T(512)(128)(4,1)} %get-tuple-element.204) | copy-start | bytes 772
  341.6 7.3 %copy-start.45 = (f32[256]{0:T(256)S(1)}, f32[256]{0:T(256)}, u32[]{:S(2)}) copy-start(f32[256]{0:T(256)} %param.23) | copy-start | bytes 3076
  (13 other events, 32.5 us)
Sparse Core Ops, SparseCore 0:
  8.9 13.2 all-gather.8
  24.3 41.4 all-gather.10
  68.0 47.7 all-gather.12
  117.8 38.7 all-gather.14
  158.6 47.7 all-gather.16
  208.4 47.6 all-gather.18
  362.3 9.2 reduce-scatter.1
where the time goes:
time: 385 us; the launch traced here: 381 us
  local copies, waits for them, and re-layouts  123 us (32%)
  waiting for transfers between devices  108 us (28%)
  blocking collectives  53 us (14%)
  other arithmetic  52.5 us (14%)
  matrix products  26.8 us (7%)
  between operations  14.5 us (4%)
    slice x60, local copies, waits for them, and re-layouts, shards(): lax.associative_scan(chain_pairs, (decays, drives), axis=0)  87.8 us
    all_gather x2, blocking collectives, carried_in(): everything = jax.tree.map(lambda part: lax.all_gather(part, axis), array)  53 us
    all_gather x1, waiting for transfers between devices, shards(): lax.all_gather(value_in, 'sp', axis=0, tiled=True)  47.2 us
    all_gather x1, waiting for transfers between devices, shards(): lax.all_gather(pool_in, 'sp', axis=0, tiled=True)  41.4 us
    pad x32, local copies, waits for them, and re-layouts, shards(): lax.associative_scan(chain_pairs, (decays, drives), axis=0)  24.2 us
    add x16, other arithmetic, chain_pairs(): second_pair[0] * first_pair[1] + second_pair[1]  17.6 us
    dot_general x2, matrix products, right_product(): lax.dot_general(left_rows, weight_rows, (((1,), (1,)), ((), ())), preferr...  13.1 us
    reduce_scatter x1, waiting for transfers between devices, shards(): lax.psum_scatter(right_product(pool_out, averaging_exit_matrix) + right_p...  9.43 us
  transfers between devices with their start and end apart: 8, of which 4 were waited for; matrix products, arithmetic and copies ran while one was open for 49% of the time, Pallas kernels for 0%

commit v1 on v0

v1 whole, which is shorter than its diff:
```python
import functools

import jax
import jax.numpy as jnp
from jax import lax
from jax.experimental import pallas as pl
from jax.experimental.pallas import tpu as pltpu
from jax.sharding import PartitionSpec as P

GROUP_WIDTH = 128
HEAD_DIM = 64
TAPS = 4
REACH = 16
LANES = 128
TILE = 16
MESH = pl.DeviceIdType.MESH

epsilon = 1e-06
sharpness = 8.0


def sigmoid(x):
    return 1.0 / (1.0 + jnp.exp(-x))


def softplus(v):
    small = jnp.exp(-jnp.abs(v))
    above = 1.0 + small
    gap = above - 1.0
    safe = jnp.where(gap == 0.0, 1.0, gap)
    log1p = jnp.where(gap == 0.0, small, jnp.log(above) * small / safe)
    return jnp.maximum(v, 0.0) + log1p


def one_minus_exp(y, exp_y):
    series = 1.0 + y * (1.0 / 8.0)
    for k in range(7, 1, -1):
        series = 1.0 + y * (1.0 / k) * series
    return jnp.where(y > -0.5, -y * series, 1.0 - exp_y)


def gelu(x):
    return 0.5 * x * (1.0 + jnp.tanh(0.7978845608028654 * (x + 0.044715 * x * x * x)))


def layer(
    sizes,
    tokens, gain, pool_in, gate_in, value_in, pool_mix, averaging, taps, rate_mix, input_mix,
    log_rate, shift, initial, out_pool, out_rnn,
    o_ref,
    other_tokens, normed, held_in, held_out, acc, ppad, vpad, edge_out, edge_got, cum, loc,
    ends, ends_got, mix, own_sum, sum_out, sum_got,
    local_sem, ring_send, ring_recv, cross_send, cross_recv, tok_sem, edge_sem,
    end_send, end_recv, sum_send, sum_recv,
):
    n, fs, tp = sizes
    s = lax.axis_index("sp")
    f = lax.axis_index("fs")
    t = lax.axis_index("tp")
    depth = pool_in.shape[0]
    pool_width = pool_in.shape[1]
    rnn_width = gate_in.shape[1]
    half_rows = tokens.shape[0]
    rows = half_rows * tp
    other = 1 - t
    if n % 2 == 0:
        place = jnp.where(s % 2 == 0, s // 2, n - 1 - s // 2)

        def at_place(p):
            p = (p + 2 * n) % n
            return jnp.where(p < n // 2, 2 * p, 2 * (n - 1 - p) + 1)
    else:
        place = s

        def at_place(p):
            return (p + 2 * n) % n

    right, left = at_place(place + 1), at_place(place - 1)
    crossing = fs == 2
    if crossing:
        part = depth // 3 // TILE * TILE
        common = depth - 2 * part
        e_start = pl.multiple_of(f * (part + common), TILE)
        x_start = pl.multiple_of((1 - f) * (part + common), TILE)
        a_start = part
    else:
        part = depth // 2
        common = depth - part
        e_start, a_start, x_start = 0, part, 0
    pieces = (pl.ds(e_start, part), pl.ds(a_start, common))
    far = n // 2
    pending = []

    barrier = pltpu.get_barrier_semaphore()
    copies = []
    for k, (src, dst) in enumerate((
        (pool_in, held_in.at[s, :, pl.ds(0, pool_width)]),
        (gate_in, held_in.at[s, :, pl.ds(pool_width, rnn_width)]),
        (value_in, held_in.at[s, :, pl.ds(pool_width + rnn_width, rnn_width)]),
        (out_pool, held_out.at[s, :, pl.ds(0, pool_width)]),
        (out_rnn, held_out.at[s, :, pl.ds(pool_width, rnn_width)]),
    )):
        copy = pltpu.make_async_copy(src, dst, local_sem.at[k])
        copy.start()
        copies.append(copy)
    for k in range(1, n):
        pl.semaphore_signal(barrier, inc=1, device_id={"sp": (s + k) % n}, device_id_type=MESH)
    pl.semaphore_signal(barrier, inc=1, device_id={"tp": other}, device_id_type=MESH)
    if crossing:
        pl.semaphore_signal(barrier, inc=1, device_id={"fs": 1 - f}, device_id_type=MESH)
    pl.semaphore_wait(barrier, n + (1 if crossing else 0))

    held = (held_in, held_out)

    def carried(d, way):
        if 2 * d == n:
            return (way,)
        return (0, 1)

    def send(stream, d, way, piece, block):
        ref = held[stream].at[block, pieces[piece], :]
        copy = pltpu.make_async_remote_copy(
            src_ref=ref, dst_ref=ref,
            send_sem=ring_send.at[stream, d, way, piece],
            recv_sem=ring_recv.at[stream, d, way, piece],
            device_id={"sp": right if way == 0 else left}, device_id_type=MESH,
        )
        copy.start()
        pending.append(copy)

    def ring_descriptor(stream, d, way, piece, block):
        ref = held[stream].at[block, pieces[piece], :]
        return pltpu.make_async_remote_copy(
            src_ref=ref, dst_ref=ref,
            send_sem=ring_send.at[stream, d, way, piece],
            recv_sem=ring_recv.at[stream, d, way, piece],
            device_id={"sp": right if way == 0 else left}, device_id_type=MESH,
        )

    def block_at(d, way):
        return at_place(place - d) if way == 0 else at_place(place + d)

    def start_ring(stream):
        for piece in (0, 1):
            for way in (0, 1):
                if piece in carried(1, way):
                    send(stream, 1, way, piece, s)

    def ring_step(stream, d):
        for piece in (0, 1):
            for way in (0, 1):
                if piece not in carried(d, way):
                    continue
                block = block_at(d, way)
                ring_descriptor(stream, d, way, piece, block).wait_recv()
                if d < far and piece in carried(d + 1, way):
                    send(stream, d + 1, way, piece, block)
                if crossing and piece == 0:
                    ref = held[stream].at[block, pieces[0], :]
                    copy = pltpu.make_async_remote_copy(
                        src_ref=ref, dst_ref=ref,
                        send_sem=cross_send.at[stream, d, way],
                        recv_sem=cross_recv.at[stream, d, way],
                        device_id={"fs": 1 - f}, device_id_type=MESH,
                    )
                    copy.start()
                    pending.append(copy)

    def blocks_of(stream, d):
        result = []
        for way in (0, 1):
            if 2 * d == n and way == 1:
                continue
            block = block_at(d, way)
            if crossing:
                ref = held[stream].at[block, pl.ds(x_start, part), :]
                pltpu.make_async_remote_copy(
                    src_ref=ref, dst_ref=ref,
                    send_sem=cross_send.at[stream, d, way],
                    recv_sem=cross_recv.at[stream, d, way],
                    device_id={"fs": 1 - f}, device_id_type=MESH,
                ).wait_recv()
            result.append(block)
        return result

    for copy in copies[:3]:
        copy.wait()
    if far:
        start_ring(0)
    token_copy = pltpu.make_async_remote_copy(
        src_ref=tokens, dst_ref=other_tokens, send_sem=tok_sem.at[0], recv_sem=tok_sem.at[1],
        device_id={"tp": other}, device_id_type=MESH,
    )
    token_copy.start()
    pending.append(token_copy)
    for copy in copies[3:]:
        copy.wait()

    step_rows = 32

    def normalize(source, base):
        @pl.loop(0, half_rows // step_rows)
        def _(i):
            at = pl.multiple_of(i * step_rows, step_rows)
            wide = source[pl.ds(at, step_rows), :].astype(jnp.float32)
            scale = lax.rsqrt(jnp.mean(wide * wide, axis=1, keepdims=True) + epsilon)
            result = (wide * scale * gain[...]).astype(jnp.bfloat16)
            put = pl.ds(pl.multiple_of(base + at, step_rows), step_rows)
            for b in range(n):
                normed[b, put, :] = result[:, b * depth : (b + 1) * depth]

    normalize(tokens, t * half_rows)
    token_copy.wait_recv()
    normalize(other_tokens, other * half_rows)

    total_width = acc.shape[1]
    wide_step = 256 if total_width % 256 == 0 else LANES

    def project(block, first=False):
        @pl.loop(0, total_width // wide_step)
        def _(j):
            cols = pl.ds(pl.multiple_of(j * wide_step, wide_step), wide_step)
            product = jnp.dot(
                normed[block], held_in[block, :, cols], preferred_element_type=jnp.float32
            )
            if first:
                acc[:, cols] = product
            else:
                acc[:, cols] += product

    project(s, True)
    for d in range(1, far + 1):
        if d == far:
            start_ring(1)
        ring_step(0, d)
        if d > 1:
            for block in blocks_of(0, d - 1):
                project(block)
    if far:
        for block in blocks_of(0, far):
            project(block)

    advanced = [0]

    def advance():
        if advanced[0] < far:
            advanced[0] += 1
            ring_step(1, advanced[0])

    last = pl.ds(rows - REACH, REACH)
    edge_out[:, pl.ds(0, pool_width)] = acc[last, pl.ds(0, pool_width)].astype(jnp.bfloat16)
    edge_out[:, pl.ds(pool_width, rnn_width)] = acc[
        last, pl.ds(pool_width + rnn_width, rnn_width)
    ].astype(jnp.bfloat16)
    edge_copy = pltpu.make_async_remote_copy(
        src_ref=edge_out, dst_ref=edge_got, send_sem=edge_sem.at[0], recv_sem=edge_sem.at[1],
        device_id={"sp": (s + 1) % n}, device_id_type=MESH,
    )
    edge_copy.start()
    pending.append(edge_copy)

    here = pl.ds(REACH, rows)
    for c in range(pool_width // LANES):
        cols = pl.ds(c * LANES, LANES)
        ppad[here, cols] = acc[:, cols].astype(jnp.bfloat16).astype(jnp.float32)
    for c in range(rnn_width // LANES):
        vpad[here, pl.ds(c * LANES, LANES)] = (
            acc[:, pl.ds(pool_width + rnn_width + c * LANES, LANES)]
            .astype(jnp.bfloat16).astype(jnp.float32)
        )
    edge_copy.wait_recv()
    begins = s > 0
    ppad[pl.ds(0, REACH), :] = jnp.where(
        begins, edge_got[:, pl.ds(0, pool_width)].astype(jnp.float32), 0.0
    )
    vpad[pl.ds(0, REACH), :] = jnp.where(
        begins, edge_got[:, pl.ds(pool_width, rnn_width)].astype(jnp.float32), 0.0
    )

    row_at = lax.broadcasted_iota(jnp.int32, (rows, LANES), 0)
    ends[...] = jnp.zeros_like(ends)

    @pl.loop(0, rnn_width // LANES)
    def _(c):
        cols = pl.ds(pl.multiple_of(c * LANES, LANES), LANES)
        padded = vpad[:, cols]
        conv = taps[TAPS - 1 : TAPS, cols] * padded[REACH:]
        for back in range(1, TAPS):
            conv = conv + taps[TAPS - 1 - back : TAPS - back, cols] * pltpu.roll(padded, back, 0)[REACH:]
        conv = conv.astype(jnp.bfloat16)
        wide = conv.astype(jnp.float32)
        r_at = lax.broadcasted_iota(jnp.int32, (HEAD_DIM, LANES), 0)
        c_at = lax.broadcasted_iota(jnp.int32, (HEAD_DIM, LANES), 1)
        repeat = jnp.where((c_at - r_at) % HEAD_DIM == 0, 1.0, 0.0).astype(jnp.bfloat16)
        same = (
            lax.broadcasted_iota(jnp.int32, (LANES, LANES), 0) // HEAD_DIM
            == lax.broadcasted_iota(jnp.int32, (LANES, LANES), 1) // HEAD_DIM
        )

        def gate_of(matrix):
            spread = jnp.dot(matrix[cols, :], repeat, preferred_element_type=jnp.float32)
            diagonal = jnp.where(same, spread, 0.0).astype(jnp.bfloat16)
            return sigmoid(jnp.dot(conv, diagonal, preferred_element_type=jnp.float32))

        rate = gate_of(rate_mix)
        per = LANES // HEAD_DIM
        lane_head = lax.broadcasted_iota(jnp.int32, (LANES, rows), 0) // HEAD_DIM
        across = jnp.broadcast_to(shift[pl.ds(c * per, 1), :], (LANES, rows))
        for k in range(1, per):
            across = jnp.where(lane_head == k, shift[pl.ds(c * per + k, 1), :], across)
        log_decay = -sharpness * rate * softplus(-log_rate[:, cols]) + jnp.transpose(across)
        a = jnp.exp(log_decay)
        b = jnp.sqrt(one_minus_exp(2.0 * log_decay, a * a)) * gate_of(input_mix) * wide
        step = 1
        while step < rows:
            if step < 8:
                reached = row_at >= step
                before_a = jnp.where(reached, pltpu.roll(a, step, 0), 1.0)
                before_b = jnp.where(reached, pltpu.roll(b, step, 0), 0.0)
            else:
                before_a = jnp.concatenate([jnp.ones((step, LANES), jnp.float32), a[:-step]], axis=0)
                before_b = jnp.concatenate([jnp.zeros((step, LANES), jnp.float32), b[:-step]], axis=0)
            b = b + a * before_b
            a = a * before_a
            step *= 2
        cum[:, cols] = a
        loc[:, cols] = b
        ends[0:1, cols] = a[rows - 1 : rows]
        ends[1:2, cols] = b[rows - 1 : rows]

    for k in range(1, n):
        copy = pltpu.make_async_remote_copy(
            src_ref=ends, dst_ref=ends_got.at[k], send_sem=end_send.at[k], recv_sem=end_recv.at[k],
            device_id={"sp": (s + k) % n}, device_id_type=MESH,
        )
        copy.start()
        pending.append(copy)
    advance()

    groups_here = pool_width // GROUP_WIDTH
    positions = s * rows + row_at
    for g in range(groups_here):
        cols = pl.ds(g * GROUP_WIDTH, GROUP_WIDTH)
        group = t * groups_here + g
        padded = ppad[:, cols]
        value = padded[REACH:]
        total = padded
        window_sum = jnp.zeros_like(value)
        window = 1
        k = 0
        while 2 ** (k + 1) <= REACH:
            total = total + pltpu.roll(total, 2**k, 0)
            window_sum = jnp.where(group == k, total[REACH:], window_sum)
            window = jnp.where(group == k, 2 ** (k + 1), window)
            k += 1
        counts = jnp.minimum(positions + 1, window).astype(jnp.float32)
        pooled = (window_sum / counts - value).astype(jnp.bfloat16)
        mixed = jnp.dot(pooled, pool_mix[g], preferred_element_type=jnp.float32)
        mix[:, cols] = (mixed * averaging[:, cols]).astype(jnp.bfloat16)
    advance()

    carry = initial[...]
    for k in range(n - 1, 0, -1):
        pltpu.make_async_remote_copy(
            src_ref=ends, dst_ref=ends_got.at[k], send_sem=end_send.at[k], recv_sem=end_recv.at[k],
            device_id={"sp": (s + k) % n}, device_id_type=MESH,
        ).wait_recv()
        carry = jnp.where(k <= s, ends_got[k, 0:1, :] * carry + ends_got[k, 1:2, :], carry)

    for c in range(rnn_width // LANES):
        cols = pl.ds(c * LANES, LANES)
        hidden = loc[:, cols] + cum[:, cols] * carry[:, c * LANES : (c + 1) * LANES]
        gate = acc[:, pl.ds(pool_width + c * LANES, LANES)].astype(jnp.bfloat16).astype(jnp.float32)
        mix[:, pl.ds(pool_width + c * LANES, LANES)] = (gelu(gate) * hidden).astype(jnp.bfloat16)
    advance()

    mine = pl.ds(pl.multiple_of(t * half_rows, half_rows), half_rows)
    theirs = pl.ds(pl.multiple_of(other * half_rows, half_rows), half_rows)
    dims = (((1,), (1,)), ((), ()))
    sums = []

    def sum_copy(i, block):
        return pltpu.make_async_remote_copy(
            src_ref=sum_out.at[block], dst_ref=sum_got.at[block],
            send_sem=sum_send.at[i], recv_sem=sum_recv.at[i],
            device_id={"tp": other}, device_id_type=MESH,
        )

    def produce(block):
        i = len(sums)
        sum_out[block] = lax.dot_general(
            mix[theirs, :], held_out[block], dims, preferred_element_type=jnp.float32
        ).astype(jnp.bfloat16)
        copy = sum_copy(i, block)
        copy.start()
        pending.append(copy)
        sums.append(block)
        own_sum[block] = lax.dot_general(
            mix[mine, :], held_out[block], dims, preferred_element_type=jnp.float32
        )

    produce(s)
    for d in range(1, far + 1):
        if d > advanced[0]:
            advance()
        for block in blocks_of(1, d):
            produce(block)
    aligned = depth % LANES == 0
    for i, block in enumerate(sums):
        sum_copy(i, block).wait_recv()
        if aligned:
            o_ref[:, pl.ds(pl.multiple_of(block * depth, LANES), depth)] = (
                own_sum[block] + sum_got[block].astype(jnp.float32)
            ).astype(jnp.bfloat16)
    if not aligned:
        for b in range(n):
            o_ref[:, b * depth : (b + 1) * depth] = (
                own_sum[b] + sum_got[b].astype(jnp.float32)
            ).astype(jnp.bfloat16)
    for copy in pending:
        copy.wait_send()


def shards(
    sizes,
    tokens, norm_gain, pool_in, gate_in, value_in, pool_mix, averaging_factor, conv_taps,
    rate_mix, input_mix, log_rate, decay_shift, initial_state, out_pool, out_rnn,
):
    n, fs, tp = sizes
    half_rows, width = tokens.shape
    rows = half_rows * tp
    depth, pool_width = pool_in.shape
    rnn_width = gate_in.shape[1]
    bf, f32 = jnp.bfloat16, jnp.float32
    far = n // 2
    vmem = pl.BlockSpec(memory_space=pltpu.VMEM)
    hbm = pl.BlockSpec(memory_space=pl.ANY)
    dma = pltpu.SemaphoreType.DMA
    all_in = pool_width + 2 * rnn_width
    all_out = pool_width + rnn_width
    return pl.pallas_call(
        functools.partial(layer, sizes),
        out_shape=jax.ShapeDtypeStruct((half_rows, width), bf),
        in_specs=[vmem, vmem, hbm, hbm, hbm, vmem, vmem, vmem, vmem, vmem, vmem, vmem, vmem, hbm, hbm],
        out_specs=vmem,
        scratch_shapes=[
            pltpu.VMEM((half_rows, width), bf),
            pltpu.VMEM((n, rows, depth), bf),
            pltpu.VMEM((n, depth, all_in), bf),
            pltpu.VMEM((n, depth, all_out), bf),
            pltpu.VMEM((rows, all_in), f32),
            pltpu.VMEM((REACH + rows, pool_width), f32),
            pltpu.VMEM((REACH + rows, rnn_width), f32),
            pltpu.VMEM((REACH, all_out), bf),
            pltpu.VMEM((REACH, all_out), bf),
            pltpu.VMEM((rows, rnn_width), f32),
            pltpu.VMEM((rows, rnn_width), f32),
            pltpu.VMEM((8, rnn_width), f32),
            pltpu.VMEM((n, 8, rnn_width), f32),
            pltpu.VMEM((rows, all_out), bf),
            pltpu.VMEM((n, half_rows, depth), f32),
            pltpu.VMEM((n, half_rows, depth), bf),
            pltpu.VMEM((n, half_rows, depth), bf),
            dma((5,)),
            dma((2, far + 1, 2, 2)),
            dma((2, far + 1, 2, 2)),
            dma((2, far + 1, 2)),
            dma((2, far + 1, 2)),
            dma((2,)),
            dma((2,)),
            dma((n,)),
            dma((n,)),
            dma((n,)),
            dma((n,)),
        ],
        compiler_params=pltpu.CompilerParams(
            collective_id=0, has_side_effects=True, vmem_limit_bytes=60 * 1024 * 1024
        ),
    )(
        tokens,
        norm_gain[None, :],
        pool_in,
        gate_in,
        value_in,
        pool_mix,
        averaging_factor[None, :],
        conv_taps,
        rate_mix.reshape(rnn_width, HEAD_DIM),
        input_mix.reshape(rnn_width, HEAD_DIM),
        log_rate[None, :],
        decay_shift,
        initial_state[None, :],
        out_pool,
        out_rnn,
    )


def solution(mesh):
    sizes = (mesh.shape["sp"], mesh.shape["fs"], mesh.shape["tp"])
    placed = (
        P(("fs", "sp", "tp"), None),
        P(),
        P("sp", "tp"),
        P("sp", "tp"),
        P("sp", "tp"),
        P("tp", None, None),
        P("tp"),
        P(None, "tp"),
        P("tp", None, None),
        P("tp", None, None),
        P("tp"),
        P(("fs", "tp"), "sp"),
        P(("fs", "tp")),
        P("sp", "tp"),
        P("sp", "tp"),
    )
    return jax.shard_map(
        functools.partial(shards, sizes),
        mesh=mesh,
        in_specs=placed,
        out_specs=P(("fs", "sp", "tp"), None),
        check_vma=False,
    )
```

time: 385 us -> 87.2 us (0.23)
  local copies, waits for them, and re-layouts: 123 us -> 2.3 us
  waiting for transfers between devices: 108 us -> 0 us
  Pallas kernels: 0 us -> 84.7 us
  blocking collectives: 53 us -> 0 us
  other arithmetic: 52.5 us -> 0 us
  matrix products: 26.8 us -> 0 us
  between operations: 14.5 us -> 0.01 us
    all_gather x6 -> x0, waiting for transfers between devices: 95.2 us -> none  [the longest x1 47.2 us: shards(): lax.all_gather(value_in, 'sp', axis=0, tiled=True)]
    slice x66 -> x0, local copies, waits for them, and re-layouts: 87.8 us -> none  [the longest x60 87.8 us: shards(): lax.associative_scan(chain_pairs, (decays, drives), axis=0)]
    pallas_call x0 -> x1, Pallas kernels: none -> 84.7 us  [shards(): pl.pallas_call(functools.partial(layer, sizes), out_shape=jax.ShapeDtypeS...]
    all_gather x2 -> x0, blocking collectives: 53 us -> none  [carried_in(): everything = jax.tree.map(lambda part: lax.all_gather(part, axis), array)]
    dot_general x6 -> x0, matrix products: 26.8 us -> none  [the longest x2 13.1 us: right_product(): lax.dot_general(left_rows, weight_rows, (((1,), (1,)), ((), ())), preferr...]
    pad x32 -> x0, local copies, waits for them, and re-layouts: 24.2 us -> none  [shards(): lax.associative_scan(chain_pairs, (decays, drives), axis=0)]
    add x33 -> x0, other arithmetic: 22.7 us -> none  [the longest x16 17.6 us: chain_pairs(): second_pair[0] * first_pair[1] + second_pair[1]]
    reduce_scatter x1 -> x0, waiting for transfers between devices: 9.43 us -> none  [shards(): lax.psum_scatter(right_product(pool_out, averaging_exit_matrix) + right_p...]
  transfers between devices with their start and end apart: 8 -> 0, of which waited for: 4 -> 0; matrix products, arithmetic and copies ran while one was open for 49% -> 0% of each run, Pallas kernels for 0% -> 0%
where the time goes in v1:
time: 87.2 us; the launch traced here: 87 us
  Pallas kernels  84.7 us (97%)
  local copies, waits for them, and re-layouts  2.3 us (3%)
    pallas_call x1, Pallas kernels, shards(): pl.pallas_call(functools.partial(layer, sizes), out_shape=jax.ShapeDtypeS...  84.7 us
    unnamed x1, local copies, waits for them, and re-layouts  2.3 us

profile of v1, /device:TPU:0, one launch (start us, length us, event | category | flops | bytes accessed | tf_op | source)
XLA Modules:
  0.0 87.0 jit_solution(2383665400212489756)
XLA Ops:
  0.0 84.7 %shard_map.145 = bf16[256,2048]{1,0:T(8,128)(2,1)} custom-call(bf16[256,2048]{1,0:T(8,128)(2,1)} %tokens.1, f32[1,2048]{1,0:T(1,128)} %bitcast.8, bf16[256,256]{1,0:T(8,128)(2,1)} %pool_in.1, bf16[256,512]{1,0:T(8,128)(2,1)} %gate_in.1, bf16[256,512]{1,0:T(8,128)(2,1)} %value_in.1, bf16[2,128,128]{2,1,0:T(8,128)(2,1)} %pool_mix.1, f32[1,256]{1,0:T(1,128)} %bitcast.11, ...), custom_call_target="tpu_custom_call" | custom-call | tf_op jit(solution)/shard_map/pallas_call | solution.py:441
  84.7 2.3 %copy.17 = bf16[256,2048]{1,0:T(8,128)(2,1)} copy(bf16[256,2048]{1,0:T(8,128)(2,1)} %shard_map.145) | data formatting | bytes 2097152

commit v2 on v1

--- a/solution.py
+++ b/solution.py
@@ -45,12 +45,13 @@
 
 def layer(
     sizes,
-    tokens, gain, pool_in, gate_in, value_in, pool_mix, averaging, taps, rate_mix, input_mix,
-    log_rate, shift, initial, out_pool, out_rnn,
-    o_ref,
+    tokens_hbm, gain_hbm, pool_in, gate_in, value_in, pool_mix_hbm, averaging_hbm, taps_hbm,
+    rate_mix_hbm, input_mix_hbm, log_rate_hbm, shift_hbm, initial_hbm, out_pool, out_rnn,
+    result_hbm,
+    tokens, gain, pool_mix, averaging, taps, rate_mix, input_mix, log_rate, shift, initial, o_ref,
     other_tokens, normed, held_in, held_out, acc, ppad, vpad, edge_out, edge_got, cum, loc,
     ends, ends_got, mix, own_sum, sum_out, sum_got,
-    local_sem, ring_send, ring_recv, cross_send, cross_recv, tok_sem, edge_sem,
+    local_sem, result_sem, ring_send, ring_recv, cross_send, cross_recv, tok_sem, edge_sem,
     end_send, end_recv, sum_send, sum_recv,
 ):
     n, fs, tp = sizes
@@ -92,23 +93,33 @@
     pending = []
 
     barrier = pltpu.get_barrier_semaphore()
+    for neighbour in (left, right):
+        pl.semaphore_signal(barrier, inc=1, device_id={"sp": neighbour}, device_id_type=MESH)
+    pl.semaphore_signal(barrier, inc=1, device_id={"tp": other}, device_id_type=MESH)
+    if crossing:
+        pl.semaphore_signal(barrier, inc=1, device_id={"fs": 1 - f}, device_id_type=MESH)
     copies = []
     for k, (src, dst) in enumerate((
         (pool_in, held_in.at[s, :, pl.ds(0, pool_width)]),
         (gate_in, held_in.at[s, :, pl.ds(pool_width, rnn_width)]),
         (value_in, held_in.at[s, :, pl.ds(pool_width + rnn_width, rnn_width)]),
+        (tokens_hbm, tokens),
+        (gain_hbm, gain),
         (out_pool, held_out.at[s, :, pl.ds(0, pool_width)]),
         (out_rnn, held_out.at[s, :, pl.ds(pool_width, rnn_width)]),
+        (pool_mix_hbm, pool_mix),
+        (averaging_hbm, averaging),
+        (taps_hbm, taps),
+        (rate_mix_hbm, rate_mix),
+        (input_mix_hbm, input_mix),
+        (log_rate_hbm, log_rate),
+        (shift_hbm, shift),
+        (initial_hbm, initial),
     )):
         copy = pltpu.make_async_copy(src, dst, local_sem.at[k])
         copy.start()
         copies.append(copy)
-    for k in range(1, n):
-        pl.semaphore_signal(barrier, inc=1, device_id={"sp": (s + k) % n}, device_id_type=MESH)
-    pl.semaphore_signal(barrier, inc=1, device_id={"tp": other}, device_id_type=MESH)
-    if crossing:
-        pl.semaphore_signal(barrier, inc=1, device_id={"fs": 1 - f}, device_id_type=MESH)
-    pl.semaphore_wait(barrier, n + (1 if crossing else 0))
+    pl.semaphore_wait(barrier, 4 if crossing else 3)
 
     held = (held_in, held_out)
 
@@ -187,14 +198,14 @@
         copy.wait()
     if far:
         start_ring(0)
+    for copy in copies[3:5]:
+        copy.wait()
     token_copy = pltpu.make_async_remote_copy(
         src_ref=tokens, dst_ref=other_tokens, send_sem=tok_sem.at[0], recv_sem=tok_sem.at[1],
         device_id={"tp": other}, device_id_type=MESH,
     )
     token_copy.start()
     pending.append(token_copy)
-    for copy in copies[3:]:
-        copy.wait()
 
     step_rows = 32
 
@@ -229,6 +240,8 @@
                 acc[:, cols] += product
 
     project(s, True)
+    for copy in copies[5:]:
+        copy.wait()
     for d in range(1, far + 1):
         if d == far:
             start_ring(1)
@@ -280,8 +293,7 @@
     row_at = lax.broadcasted_iota(jnp.int32, (rows, LANES), 0)
     ends[...] = jnp.zeros_like(ends)
 
-    @pl.loop(0, rnn_width // LANES)
-    def _(c):
+    def recur(c):
         cols = pl.ds(pl.multiple_of(c * LANES, LANES), LANES)
         padded = vpad[:, cols]
         conv = taps[TAPS - 1 : TAPS, cols] * padded[REACH:]
@@ -328,6 +340,11 @@
         ends[0:1, cols] = a[rows - 1 : rows]
         ends[1:2, cols] = b[rows - 1 : rows]
 
+    chunks = rnn_width // LANES
+    pl.loop(0, chunks // 2)(recur)
+    advance()
+    pl.loop(chunks // 2, chunks)(recur)
+
     for k in range(1, n):
         copy = pltpu.make_async_remote_copy(
             src_ref=ends, dst_ref=ends_got.at[k], send_sem=end_send.at[k], recv_sem=end_recv.at[k],
@@ -406,19 +423,31 @@
         for block in blocks_of(1, d):
             produce(block)
     aligned = depth % LANES == 0
+    results = []
     for i, block in enumerate(sums):
         sum_copy(i, block).wait_recv()
         if aligned:
             o_ref[:, pl.ds(pl.multiple_of(block * depth, LANES), depth)] = (
                 own_sum[block] + sum_got[block].astype(jnp.float32)
             ).astype(jnp.bfloat16)
+            columns = pl.ds(pl.multiple_of(block * depth, LANES), depth)
+            copy = pltpu.make_async_copy(
+                o_ref.at[:, columns], result_hbm.at[:, columns], result_sem.at[i]
+            )
+            copy.start()
+            results.append(copy)
     if not aligned:
         for b in range(n):
             o_ref[:, b * depth : (b + 1) * depth] = (
                 own_sum[b] + sum_got[b].astype(jnp.float32)
             ).astype(jnp.bfloat16)
+        copy = pltpu.make_async_copy(o_ref, result_hbm, result_sem.at[0])
+        copy.start()
+        results.append(copy)
     for copy in pending:
         copy.wait_send()
+    for copy in results:
+        copy.wait()
 
 
 def shards(
@@ -433,7 +462,6 @@
     rnn_width = gate_in.shape[1]
     bf, f32 = jnp.bfloat16, jnp.float32
     far = n // 2
-    vmem = pl.BlockSpec(memory_space=pltpu.VMEM)
     hbm = pl.BlockSpec(memory_space=pl.ANY)
     dma = pltpu.SemaphoreType.DMA
     all_in = pool_width + 2 * rnn_width
@@ -441,9 +469,20 @@
     return pl.pallas_call(
         functools.partial(layer, sizes),
         out_shape=jax.ShapeDtypeStruct((half_rows, width), bf),
-        in_specs=[vmem, vmem, hbm, hbm, hbm, vmem, vmem, vmem, vmem, vmem, vmem, vmem, vmem, hbm, hbm],
-        out_specs=vmem,
+        in_specs=[hbm] * 15,
+        out_specs=hbm,
         scratch_shapes=[
+            pltpu.VMEM((half_rows, width), bf),
+            pltpu.VMEM((1, width), f32),
+            pltpu.VMEM(pool_mix.shape, bf),
+            pltpu.VMEM((1, pool_width), f32),
+            pltpu.VMEM(conv_taps.shape, f32),
+            pltpu.VMEM((rnn_width, HEAD_DIM), bf),
+            pltpu.VMEM((rnn_width, HEAD_DIM), bf),
+            pltpu.VMEM((1, rnn_width), f32),
+            pltpu.VMEM(decay_shift.shape, f32),
+            pltpu.VMEM((1, rnn_width), f32),
+            pltpu.VMEM((half_rows, width), bf),
             pltpu.VMEM((half_rows, width), bf),
             pltpu.VMEM((n, rows, depth), bf),
             pltpu.VMEM((n, depth, all_in), bf),
@@ -461,7 +500,8 @@
             pltpu.VMEM((n, half_rows, depth), f32),
             pltpu.VMEM((n, half_rows, depth), bf),
             pltpu.VMEM((n, half_rows, depth), bf),
-            dma((5,)),
+            dma((15,)),
+            dma((n,)),
             dma((2, far + 1, 2, 2)),
             dma((2, far + 1, 2, 2)),
             dma((2, far + 1, 2)),

time: 87.2 us -> 81.7 us (0.937)
  Pallas kernels: 84.7 us -> 79.1 us
    pallas_call x1, Pallas kernels: 84.7 us -> 79.1 us  [shards(): pl.pallas_call(functools.partial(layer, sizes), out_shape=jax.ShapeDtypeS...]
where the time goes in v2:
time: 81.7 us; the launch traced here: 81.4 us
  Pallas kernels  79.1 us (97%)
  local copies, waits for them, and re-layouts  2.3 us (3%)
    pallas_call x1, Pallas kernels, shards(): pl.pallas_call(functools.partial(layer, sizes), out_shape=jax.ShapeDtypeS...  79.1 us
    unnamed x1, local copies, waits for them, and re-layouts  2.3 us

profile of v2, /device:TPU:0, one launch (start us, length us, event | category | flops | bytes accessed | tf_op | source)
XLA Modules:
  0.0 81.4 jit_solution(4638385561803739966)
XLA Ops:
  0.0 79.1 %shard_map.145 = bf16[256,2048]{1,0:T(8,128)(2,1)} custom-call(bf16[256,2048]{1,0:T(8,128)(2,1)} %tokens_hbm.1, f32[1,2048]{1,0:T(1,128)} %bitcast.8, bf16[256,256]{1,0:T(8,128)(2,1)} %pool_in.1, bf16[256,512]{1,0:T(8,128)(2,1)} %gate_in.1, bf16[256,512]{1,0:T(8,128)(2,1)} %value_in.1, bf16[2,128,128]{2,1,0:T(8,128)(2,1)} %pool_mix_hbm.1, ...), custom_call_target="tpu_custom_call" | custom-call | tf_op jit(solution)/shard_map/pallas_call | solution.py:469
  79.1 2.3 %copy.17 = bf16[256,2048]{1,0:T(8,128)(2,1)} copy(bf16[256,2048]{1,0:T(8,128)(2,1)} %shard_map.145) | data formatting | bytes 2097152
